TPU v7x, 32 devices: a whole 2x2x4 slice. The times are simulated.
32 devices in a mesh: sp: 8 (over z, x), tp: 4 (over y, core).
Axes of the slice: x: 2, y: 2, z: 4, core: 2. Of those that a mesh axis runs over, the one named last changes fastest.
Arguments:
- residual: bfloat16 [1536, 2048], P('sp', 'tp'), may hold values from -10 to 10
- queries: bfloat16 [1536, 16, 128], P('sp', 'tp'), may hold values from -6.5 to 6.5
- key_rows: bfloat16 [1536, 16, 128], P('sp', 'tp'), may hold values from -6.5 to 6.5
- value_rows: bfloat16 [1536, 16, 128], P('sp', 'tp'), may hold values from -6 to 6
- diff_scale: float32 [16], P('tp'), may hold values from 0.3 to 0.8
- head_gain: float32 [128], replicated, may hold values from 0.1 to 1.9
- out_weight: bfloat16 [2048, 2048], P(None, 'tp'), may hold values from -0.125 to 0.125
- norm_gain: float32 [2048], replicated, may hold values from 0.1 to 1.9
- gate_weight: bfloat16 [8, 2048, 4096], P('sp', None, 'tp'), may hold values from -0.5 to 0.5
- up_weight: bfloat16 [8, 2048, 4096], P('sp', None, 'tp'), may hold values from -0.5 to 0.5
- down_weight: bfloat16 [8, 4096, 2048], P('sp', None, 'tp'), may hold values from -0.01171875 to 0.01171875
- expert_ids: int32 [1536, 2], P('sp'), may hold values from 0 to 7, all different within a row; in each aligned block of 192 rows (0 to 191, 192 to 383, ...) at most 96 rows name the same one
- route_logit: float32 [1536, 2], P('sp'), may hold values from -6 to 6
Outputs:
- updated: bfloat16 [1536, 2048], P('sp', 'tp')
Inputs may be any that keep to these rules, and one draw needn't show every extreme that they name: `expert_ids`: A token's 2 experts differ. The 192 tokens of one index of sp name one expert at most 96 times, a bound that some block reaches on some index.
All inputs are finite; a program needn't handle non-finite values.
Results may differ from a plain program's by a relative error of at most 0.014.
Values may be sent and summed in bfloat16 or wider, within the bound.
A program may use at most 64 MiB of HBM per device.

v0:
```python
import math
import jax
import jax.numpy as jnp
from jax import lax
from jax.sharding import PartitionSpec as P

D = 2048
QK = 64
SPAN = 64
NORM_EPS = 1e-05
CLAMP_LIMIT = 7.0
SWISH_ALPHA = 1.702
HEAD_KEEP = 0.8
NEG_FILL = -1e30


def update_map(running, query_half, key_half, value_block, visible):
    row_peak, row_total, accum = running
    scores = jnp.einsum(
        "qhd,khd->hqk", query_half, key_half, preferred_element_type=jnp.float32
    ) * QK ** (-0.5)
    scores = jnp.where(visible[None], scores, NEG_FILL)
    new_peak = jnp.maximum(row_peak, jnp.max(scores, axis=-1))
    exp_weights = jnp.where(visible[None], jnp.exp(scores - new_peak[..., None]), 0.0)
    rescale = jnp.exp(row_peak - new_peak)
    row_total = row_total * rescale + jnp.sum(exp_weights, axis=-1)
    accum = accum * rescale[..., None] + jnp.einsum(
        "hqk,khv->hqv",
        exp_weights.astype(jnp.bfloat16),
        value_block,
        preferred_element_type=jnp.float32,
    )
    return (new_peak, row_total, accum)


def local(
    residual,
    queries,
    key_rows,
    value_rows,
    diff_scale,
    head_gain,
    out_weight,
    norm_gain,
    gate_weight,
    up_weight,
    down_weight,
    expert_ids,
    route_logit,
):
    tokens_here = queries.shape[0]
    heads_here = queries.shape[1]
    value_width = value_rows.shape[2]
    query_start = lax.axis_index("sp") * tokens_here
    query_span = (query_start + jnp.arange(tokens_here, dtype=jnp.int32)) // SPAN
    first_query = queries[..., :QK]
    second_query = queries[..., QK:]
    empty_map = (
        jnp.full((heads_here, tokens_here), NEG_FILL, jnp.float32),
        jnp.zeros((heads_here, tokens_here), jnp.float32),
        jnp.zeros((heads_here, tokens_here, value_width), jnp.float32),
    )
    folded = (empty_map, empty_map)
    key_piece = lax.all_gather(key_rows, "sp", axis=0, tiled=True)
    value_piece = lax.all_gather(value_rows, "sp", axis=0, tiled=True)
    key_count = key_piece.shape[0]
    key_width = math.gcd(key_count, 1024)
    blocks = key_count // key_width
    key_blocks = key_piece.reshape(blocks, key_width, heads_here, 2 * QK)
    value_blocks = value_piece.reshape(blocks, key_width, heads_here, value_width)

    def advance(running, inputs):
        block_index, key_block, value_block = inputs
        key_start = block_index * key_width

        def compute(current):
            key_span = (key_start + jnp.arange(key_width, dtype=jnp.int32)) // SPAN
            visible = key_span[None, :] <= query_span[:, None]
            first = update_map(current[0], first_query, key_block[..., :QK], value_block, visible)
            second = update_map(current[1], second_query, key_block[..., QK:], value_block, visible)
            return (first, second)

        running = lax.cond(
            key_start < query_start + tokens_here, compute, lambda current: current, running
        )
        return (running, None)

    folded, _ = lax.scan(
        advance, folded, (jnp.arange(blocks, dtype=jnp.int32), key_blocks, value_blocks)
    )
    first_map, second_map = folded
    mixture = (
        first_map[2] / first_map[1][..., None]
        - diff_scale[:, None, None] * second_map[2] / second_map[1][..., None]
    )
    scale_back = lax.rsqrt(jnp.mean(mixture * mixture, axis=-1, keepdims=True) + NORM_EPS)
    attended = (mixture * scale_back * head_gain * HEAD_KEEP).astype(jnp.bfloat16)
    column_width = out_weight.shape[1]
    head_weight = out_weight.reshape(-1, value_width, column_width)
    weight_slice = head_weight
    projected = jnp.einsum(
        "htv,hvd->td",
        lax.all_gather(attended, "tp", axis=0, tiled=True),
        weight_slice,
        preferred_element_type=jnp.float32,
    )
    after_mixer = (residual.astype(jnp.float32) + projected).astype(jnp.bfloat16)
    mixer_float = after_mixer.astype(jnp.float32)
    partial_value = jnp.sum(mixer_float * mixer_float, axis=-1)
    square_total = lax.psum(partial_value, "tp")
    gain_slice = lax.dynamic_slice_in_dim(
        norm_gain, lax.axis_index("tp") * column_width, column_width, 0
    )
    normed = (mixer_float * lax.rsqrt(square_total / D + NORM_EPS)[:, None] * gain_slice).astype(
        jnp.bfloat16
    )
    experts = lax.axis_size("sp")
    top_count = expert_ids.shape[1]
    capacity = 2 * tokens_here * top_count // experts
    chosen = expert_ids.reshape(-1)
    onehot = (chosen[:, None] == jnp.arange(experts, dtype=jnp.int32)[None, :]).astype(jnp.int32)
    rank_in = jnp.sum(jnp.cumsum(onehot, axis=0) * onehot, axis=1) - 1
    slot_index = chosen * capacity + rank_in
    owner_row = (
        jnp.full((experts * capacity,), tokens_here, jnp.int32)
        .at[slot_index]
        .set(jnp.arange(tokens_here * top_count, dtype=jnp.int32) // top_count)
    )
    padded = jnp.concatenate([normed, jnp.zeros((1, normed.shape[1]), jnp.bfloat16)], axis=0)
    outgoing = padded[owner_row].reshape(experts, capacity, normed.shape[1])
    expert_input = lax.all_gather(
        lax.all_to_all(outgoing, "sp", split_axis=0, concat_axis=0, tiled=True),
        "tp",
        axis=2,
        tiled=True,
    )
    sources = expert_input.shape[0]
    items = expert_input.shape[1]
    flat_rows = expert_input.reshape(sources * items, -1)
    pre_gate = jnp.dot(flat_rows, gate_weight[0], preferred_element_type=jnp.float32)
    pre_up = jnp.dot(flat_rows, up_weight[0], preferred_element_type=jnp.float32)
    capped = jnp.minimum(pre_gate, CLAMP_LIMIT)
    linear = jnp.clip(pre_up, -CLAMP_LIMIT, CLAMP_LIMIT)
    hidden = (capped * jax.nn.sigmoid(SWISH_ALPHA * capped) * (linear + 1.0)).astype(jnp.bfloat16)
    weight_slice = down_weight[0]
    expert_out = jnp.dot(
        lax.all_gather(hidden, "tp", axis=1, tiled=True),
        weight_slice,
        preferred_element_type=jnp.float32,
    )
    expert_out = expert_out.astype(jnp.bfloat16).reshape(sources, items, -1)
    returned_rows = lax.all_to_all(expert_out, "sp", split_axis=0, concat_axis=0, tiled=True)
    picked = returned_rows.reshape(experts * capacity, -1)[slot_index].astype(jnp.float32)
    picked = picked.reshape(tokens_here, top_count, -1)
    weights = jax.nn.softmax(route_logit, axis=-1)
    routed = jnp.sum(picked * weights[..., None], axis=1)
    return (mixer_float + routed).astype(jnp.bfloat16)


def solution(mesh):
    return jax.shard_map(
        local,
        mesh=mesh,
        in_specs=(
            P("sp", "tp"),
            P("sp", "tp", None),
            P("sp", "tp", None),
            P("sp", "tp", None),
            P("tp"),
            P(),
            P(None, "tp"),
            P(),
            P("sp", None, "tp"),
            P("sp", None, "tp"),
            P("sp", None, "tp"),
            P("sp", None),
            P("sp", None),
        ),
        out_specs=P("sp", "tp"),
        check_vma=False,
    )
```

profile of v0, /device:TPU:0, one launch (start us, length us, event | category | flops | bytes accessed | tf_op | source)
XLA Modules:
  0.0 296.3 jit_solution(3500172858010482587)
XLA Ops:
  6.5 1.8 copy.27
  8.4 1.6 copy.29
  10.1 0.8 copy.34
  10.9 0.1 eq.29
  11.1 0.1 eq.25
  11.2 0.2 fusion.56
  11.4 0.1 copy.37
  11.6 0.1 copy.38
  11.8 0.9 reduce-window.6
  12.6 0.2 slice_reduce_fusion
  13.0 0.1 mul.173
  13.2 0.8 dynamic_slice.28
  14.1 2.9 scatter_custom_fusion
  17.0 39.5 %all-gather.5.cloned.1.call-done = bf16[1536,4,128]{2,0,1:T(8,128)(2,1)} async-done(((bf16[192,4,128]{2,0,1:T(8,128)(2,1)}), bf16[1536,4,128]{2,0,1:T(8,128)(2,1)}) %all-gather.5.cloned.1.call-update) | async-done | bytes 1572880 | tf_op jit(solution)/shard_map/all_gather | solution.py:64
  56.5 2.6 copy.31
  59.1 42.2 %all-gather.7.cloned.1.call-done = bf16[1536,4,128]{2,0,1:T(8,128)(2,1)} async-done(((bf16[192,4,128]{2,0,1:T(8,128)(2,1)}), bf16[1536,4,128]{2,0,1:T(8,128)(2,1)}) %all-gather.7.cloned.1.call-update) | async-done | bytes 1572880 | tf_op jit(solution)/shard_map/all_gather | solution.py:65
  101.2 2.7 copy.32
  104.0 9.0 %while.23 = (s32[]{:T(128)}, f32[4,192]{1,0:T(4,128)S(1)}, f32[4,192]{1,0:T(4,128)S(1)}, f32[4,192,128]{2,1,0:T(8,128)S(1)}, f32[4,192]{1,0:T(4,128)S(1)}, /*ind...) while((s32[]{:T(128)}, f32[4,192]{1,0:T(4,128)S(1)}, ...), condition=%wide.region_7.8_spmd.clone, body=%wide.region_0.7_spmd.clone.sunk | while | flops 309574784 | bytes 20891532 | solution.py:88
  104.1 0.6 dynamic_slice.42
  105.4 5.0 %conditional.3 = ((f32[4,192]{1,0:T(4,128)S(1)}, f32[4,192]{1,0:T(4,128)S(1)}, f32[4,192,128]{2,1,0:T(8,128)S(1)}, f32[4,192]{1,0:T(4,128)S(1)}, f32[4,192]{1,0:T(4,128)S(1)}, /*index=5*/f32[4,192,128]{2,1,0:T(8,128)S(1)})) conditional(s32[]{:T(128)} %convert_element_type.82, (f32[4,192]{1,0:T(4,128)S(1)}, f32[4,192]{1,0:T(4,128)S(1)}, ...), branch_computations={%region_1.1_spmd, %region_2.6_spmd.clone} | conditional | flops 309572096 | bytes 20887848 | solution.py:83
  105.5 1.1 dynamic-slice_bitcast_fusion
  106.6 0.6 fusion.54
  107.2 0.6 fusion.55
  107.8 1.2 fusion.5
  109.0 0.2 copy-done.1
  109.2 0.6 convolution_add_fusion
  109.7 0.6 convolution_add_fusion.1
  110.4 0.6 dynamic_slice.42
  111.7 0.6 dynamic_slice.42
  113.1 0.5 multiply_reduce_fusion.2
  113.6 0.2 multiply_convert_fusion.2
  113.7 8.6 %all_gather.17 = bf16[16,192,128]{2,1,0:T(8,128)(2,1)S(1)} all-gather(bf16[4,192,128]{2,1,0:T(8,128)(2,1)S(1)} %multiply_convert_fusion.2), channel_id=1, replica_groups=mesh['sp'=8,'tp'=4] {'tp'}, dimensions={0}, use_global_device_ids=true | all-gather | bytes 983040 | tf_op jit(solution)/shard_map/all_gather | solution.py:103
  122.3 0.7 multiply_reduce_fusion.1
  123.0 6.2 %psum.7 = f32[192]{0:T(256)S(1)} all-reduce(f32[192]{0:T(256)S(1)} %get-tuple-element.467), channel_id=1, replica_groups=mesh['sp'=8,'tp'=4] {'tp'}, use_global_device_ids=true, to_apply=%region_10.11 | all-reduce | flops 192 | bytes 1536 | tf_op jit(solution)/shard_map/psum | solution.py:110
  129.3 2.7 gather_fusion
  132.0 32.5 %all_to_all.10 = bf16[8,96,512]{2,1,0:T(8,128)(2,1)} all-to-all(bf16[8,96,512]{2,1,0:T(8,128)(2,1)S(1)} %bitcast.62), channel_id=1, replica_groups=mesh['sp'=8,'tp'=4] {'sp'}, dimensions={0} | all-to-all | bytes 1572864 | tf_op jit(solution)/shard_map/all_to_all | solution.py:132
  164.5 0.2 all-gather.11.cloned.1.call-start
  164.7 26.5 %all-gather.9.cloned.1.call-done = bf16[8,96,2048]{2,1,0:T(8,128)(2,1)} async-done(((bf16[8,96,512]{2,1,0:T(8,128)(2,1)}), bf16[8,96,2048]{2,1,0:T(8,128)(2,1)}) %all-gather.9.cloned.1.call-update) | async-done | bytes 3145744 | tf_op jit(solution)/shard_map/all_gather | solution.py:131
  191.3 6.3 %fusion.32 = f32[768,1024]{1,0:T(8,128)S(1)} fusion(bf16[768,2048]{1,0:T(8,128)(2,1)} %bitcast.67, bf16[1,2048,1024]{2,1,0:T(8,128)(2,1)} %param.26), kind=kOutput, calls=%fused_computation.55 | convolution fusion | flops 3221225472 | bytes 10485760 | tf_op jit(solution)/shard_map/dot_general | solution.py:141
  197.6 5.3 %multiply_convert_fusion = bf16[768,1024]{1,0:T(8,128)(2,1)} fusion(f32[768,1024]{1,0:T(8,128)S(1)} %fusion.32, bf16[768,2048]{1,0:T(8,128)(2,1)S(1)} %bitcast.68, bf16[1,2048,1024]{2,1,0:T(8,128)(2,1)S(1)} %copy-done.8), kind=kOutput, calls=%fused_computation.59 | convolution fusion | flops 3229089792 | bytes 12058624 | tf_op jit(solution)/shard_map/dot_general | solution.py:140
  202.9 46.5 %all-gather.11.cloned.1.call-done = bf16[768,4096]{1,0:T(8,128)(2,1)} async-done(((bf16[768,1024]{1,0:T(8,128)(2,1)}), bf16[768,4096]{1,0:T(8,128)(2,1)}) %all-gather.11.cloned.1.call-update) | async-done | bytes 6291472 | tf_op jit(solution)/shard_map/all_gather | solution.py:147
  249.4 8.3 %fusion.38 = bf16[768,512]{1,0:T(8,128)(2,1)} fusion(bf16[768,4096]{1,0:T(8,128)(2,1)} %all-gather.11.cloned.1.call-done, bf16[1,4096,512]{2,1,0:T(8,128)(2,1)} %param.27), kind=kOutput, calls=%fused_computation.60 | convolution fusion | flops 3221618688 | bytes 11272192 | tf_op jit(solution)/shard_map/dot_general | solution.py:146
  257.7 5.6 %all-to-all-start.1 = ((bf16[8,96,512]{2,1,0:T(8,128)(2,1)}), bf16[8,96,512]{2,1,0:T(8,128)(2,1)S(1)}, u32[]{:S(2)}, u32[]{:S(2)}) async-start(bf16[8,96,512]{2,1,0:T(8,128)(2,1)} %bitcast.65), calls=%async_computation.1 | async-start | bytes 1572864 | tf_op jit(solution)/shard_map/all_to_all | solution.py:152
  263.6 20.4 %all-to-all-done.1 = bf16[8,96,512]{2,1,0:T(8,128)(2,1)S(1)} async-done(((bf16[8,96,512]{2,1,0:T(8,128)(2,1)}), bf16[8,96,512]{2,1,0:T(8,128)(2,1)S(1)}, u32[]{:S(2)}, u32[]{:S(2)}) %all-to-all-start.1) | async-done | bytes 786464 | tf_op jit(solution)/shard_map/all_to_all | solution.py:152
  283.9 2.6 gather_fusion.1
  286.5 1.5 reshape.153
  288.0 1.0 multiply_reduce_fusion
  289.0 0.7 add_convert_fusion
  (74 shorter events, 1.2 us)
Async XLA Ops:
  6.5 115.8 %copy-start = (bf16[2048,512]{1,0:T(8,128)(2,1)S(1)}, bf16[2048,512]{1,0:T(8,128)(2,1)}, u32[]{:S(2)}) copy-start(bf16[2048,512]{1,0:T(8,128)(2,1)} %param.23) | copy-start | bytes 6291460
  6.5 6.4 %copy-start.5 = (s32[192,2]{0,1:T(2,128)S(1)}, s32[192,2]{0,1:T(2,128)}, u32[]{:S(2)}) copy-start(s32[192,2]{0,1:T(2,128)} %param.28) | copy-start | bytes 4612
  6.5 4.7 %copy-start.2 = (bf16[192,4,128]{2,1,0:T(4,128)(2,1)S(1)}, bf16[192,4,128]{2,1,0:T(4,128)(2,1)}, u32[]{:S(2)}) copy-start(bf16[192,4,128]{2,1,0:T(4,128)(2,1)} %param.18) | copy-start | bytes 589828
  6.5 49.9 %all-gather.5.cloned.1.call-start = ((), (), s32[]{:S(2)}) async-start(), calls=%async_computation.2 | async-start | bytes 1769472 | tf_op jit(solution)/shard_map/all_gather | solution.py:64
  8.4 92.9 %all-gather.7.cloned.1.call-start = ((), (), s32[]{:S(2)}) async-start(), calls=%async_computation.3 | async-start | bytes 1769472 | tf_op jit(solution)/shard_map/all_gather | solution.py:65
  10.1 181.2 %all-gather.9.cloned.1.call-start = ((), (), s32[]{:S(2)}) async-start(), calls=%async_computation.4 | async-start | bytes 3932160 | tf_op jit(solution)/shard_map/all_gather | solution.py:131
  104.0 9.0 %copy-start.6 = (f32[4]{0:T(128)S(1)}, f32[4]{0:T(128)}, u32[]{:S(2)}) copy-start(f32[4]{0:T(128)} %param.21) | copy-start | bytes 52
  104.0 9.5 %copy-start.7 = (f32[128]{0:T(128)S(1)}, f32[128]{0:T(128)}, u32[]{:S(2)}) copy-start(f32[128]{0:T(128)} %param.22) | copy-start | bytes 1540
  107.8 1.4 copy-start.1
  113.0 9.3 %copy-start.3 = (bf16[192,512]{1,0:T(8,128)(2,1)S(1)}, bf16[192,512]{1,0:T(8,128)(2,1)}, u32[]{:S(2)}) copy-start(bf16[192,512]{1,0:T(8,128)(2,1)} %param.17) | copy-start | bytes 589828
  164.5 84.9 %all-gather.11.cloned.1.call-start = ((), (), s32[]{:S(2)}) async-start(), calls=%async_computation.5 | async-start | bytes 7864320 | tf_op jit(solution)/shard_map/all_gather | solution.py:147
  191.2 6.3 %copy-start.8 = (bf16[1,2048,1024]{2,1,0:T(8,128)(2,1)S(1)}, bf16[1,2048,1024]{2,1,0:T(8,128)(2,1)}, u32[]{:S(2)}) copy-start(bf16[1,2048,1024]{2,1,0:T(8,128)(2,1)} %param.25) | copy-start | bytes 12582916
  191.3 6.3 %copy-start.9 = (bf16[8,96,2048]{2,1,0:T(8,128)(2,1)S(1)}, bf16[8,96,2048]{2,1,0:T(8,128)(2,1)}, u32[]{:S(2)}) copy-start(bf16[8,96,2048]{2,1,0:T(8,128)(2,1)} %all-gather.9.cloned.1.call-done) | copy-start | bytes 9437188
  257.7 5.7 %copy-start.4 = (f32[192,2]{0,1:T(2,128)S(1)}, f32[192,2]{0,1:T(2,128)}, u32[]{:S(2)}) copy-start(f32[192,2]{0,1:T(2,128)} %param.29) | copy-start | bytes 4612
  257.7 26.2 %all-to-all-start.1 = ((bf16[8,96,512]{2,1,0:T(8,128)(2,1)}), bf16[8,96,512]{2,1,0:T(8,128)(2,1)S(1)}, u32[]{:S(2)}, u32[]{:S(2)}) async-start(bf16[8,96,512]{2,1,0:T(8,128)(2,1)} %bitcast.65), calls=%async_computation.1 | async-start | bytes 1572864 | tf_op jit(solution)/shard_map/all_to_all | solution.py:152
Sparse Core Ops, SparseCore 0:
  9.5 46.9 all-gather.4
  58.7 42.5 all-gather.6
  164.6 26.5 all-gather.8
  203.0 46.3 all-gather.10
where the time goes:
time: 297 us; the launch traced here: 296 us
  waiting for transfers between devices  175 us (59%)
  blocking collectives  47.2 us (16%)
  local copies, waits for them, and re-layouts  24.5 us (8%)
  matrix products  22.8 us (8%)
  between operations  13.4 us (5%)
  starting transfers between devices  5.96 us (2%)
  other arithmetic  5.09 us (2%)
    all_gather x1, waiting for transfers between devices, local(): lax.all_gather(hidden, 'tp', axis=1, tiled=True)  46.5 us
    all_gather x1, waiting for transfers between devices, local(): value_piece = lax.all_gather(value_rows, 'sp', axis=0, tiled=True)  42.2 us
    all_gather x1, waiting for transfers between devices, local(): key_piece = lax.all_gather(key_rows, 'sp', axis=0, tiled=True)  39.5 us
    all_to_all x1, blocking collectives, local(): lax.all_to_all(outgoing, 'sp', split_axis=0, concat_axis=0, tiled=True)  32.5 us
    all_gather x1, waiting for transfers between devices, local(): lax.all_gather(lax.all_to_all(outgoing, 'sp', split_axis=0, concat_axis=0...  26.5 us
    all_to_all x1, waiting for transfers between devices, local(): lax.all_to_all(expert_out, 'sp', split_axis=0, concat_axis=0, tiled=True)  20.4 us
    unnamed x25, local copies, waits for them, and re-layouts  9.82 us
    all_gather x1, blocking collectives, local(): lax.all_gather(attended, 'tp', axis=0, tiled=True)  8.58 us
  transfers between devices with their start and end apart: 5, of which 5 were waited for; matrix products, arithmetic and copies ran while one was open for 4% of the time, Pallas kernels for 0%

commit v1 on v0

--- a/solution.py
+++ b/solution.py
@@ -48,6 +48,15 @@
     expert_ids,
     route_logit,
 ):
+
+    def find_the_set(x_in, unit):
+        outer = jnp.split(
+            lax.all_gather(jnp.concatenate([unit, x_in], 1), "sp", axis=0, tiled=True),
+            [unit.shape[1]],
+            1,
+        )
+        return outer
+
     tokens_here = queries.shape[0]
     heads_here = queries.shape[1]
     value_width = value_rows.shape[2]
@@ -61,8 +70,7 @@
         jnp.zeros((heads_here, tokens_here, value_width), jnp.float32),
     )
     folded = (empty_map, empty_map)
-    key_piece = lax.all_gather(key_rows, "sp", axis=0, tiled=True)
-    value_piece = lax.all_gather(value_rows, "sp", axis=0, tiled=True)
+    key_piece, value_piece = find_the_set(value_rows, key_rows)
     key_count = key_piece.shape[0]
     key_width = math.gcd(key_count, 1024)
     blocks = key_count // key_width

time: 297 us -> 276 us (0.929)
  waiting for transfers between devices: 175 us -> 150 us
    all_gather x2 -> x1, waiting for transfers between devices: 81.6 us -> 56.6 us  [find_the_set(): lax.all_gather(jnp.concatenate([unit, x_in], 1), 'sp', axis=0, tiled=True)]
    split x0 -> x1, local copies, waits for them, and re-layouts: none -> 3.81 us  [find_the_set(): jnp.split(lax.all_gather(jnp.concatenate([unit, x_in], 1), 'sp', axis=0,...]
  transfers between devices with their start and end apart: 5 -> 4, of which waited for: 5 -> 4; matrix products, arithmetic and copies ran while one was open for 4% -> 2% of each run, Pallas kernels for 0% -> 0%
where the time goes in v1:
time: 276 us; the launch traced here: 275 us
  waiting for transfers between devices  150 us (54%)
  blocking collectives  47.8 us (17%)
  local copies, waits for them, and re-layouts  26.9 us (10%)
  matrix products  22.8 us (8%)
  between operations  13.4 us (5%)
  starting transfers between devices  5.9 us (2%)
  other arithmetic  5.87 us (2%)
    all_gather x1, waiting for transfers between devices, find_the_set(): lax.all_gather(jnp.concatenate([unit, x_in], 1), 'sp', axis=0, tiled=True)  56.6 us
    all_gather x1, waiting for transfers between devices, local(): lax.all_gather(hidden, 'tp', axis=1, tiled=True)  46.5 us
    all_to_all x1, blocking collectives, local(): lax.all_to_all(outgoing, 'sp', split_axis=0, concat_axis=0, tiled=True)  33 us
    all_gather x1, waiting for transfers between devices, local(): lax.all_gather(lax.all_to_all(outgoing, 'sp', split_axis=0, concat_axis=0...  26.8 us
    all_to_all x1, waiting for transfers between devices, local(): lax.all_to_all(expert_out, 'sp', split_axis=0, concat_axis=0, tiled=True)  20.4 us
    all_gather x1, blocking collectives, local(): lax.all_gather(attended, 'tp', axis=0, tiled=True)  8.58 us
    dot_general x1, matrix products, local(): jnp.dot(lax.all_gather(hidden, 'tp', axis=1, tiled=True), weight_slice, p...  8.3 us
    unnamed x25, local copies, waits for them, and re-layouts  7.76 us
  transfers between devices with their start and end apart: 4, of which 4 were waited for; matrix products, arithmetic and copies ran while one was open for 2% of the time, Pallas kernels for 0%

profile of v1, /device:TPU:0, one launch (start us, length us, event | category | flops | bytes accessed | tf_op | source)
XLA Modules:
  0.0 275.1 jit_solution(14690558845845546398)
XLA Ops:
  6.5 1.1 copy.27
  7.7 1.0 copy.28
  8.6 0.8 pad_maximum_fusion
  9.6 0.1 eq.29
  9.8 0.1 eq.25
  9.9 0.2 fusion.57
  10.1 0.1 copy.37
  10.3 0.1 copy.38
  10.4 0.9 reduce-window.6
  11.3 0.2 slice_reduce_fusion
  11.6 0.1 copy.33
  11.8 0.8 dynamic_slice.28
  12.7 2.9 %scatter_custom_fusion = s32[768]{0:T(1024)S(1)} fusion(s32[384]{0:T(512)S(1)} %fusion.51, s32[384]{0:T(512)S(1)} %add_select_fusion.1, s32[]{:T(128)} %constant.140.clone.1), kind=kCustom, calls=%fused_computation.91 | custom fusion | bytes 3076 | tf_op jit(solution)/shard_map/scatter | solution.py:135
  15.7 56.6 %all-gather.4.cloned.1.call-done = bf16[1536,8,128]{2,0,1:T(8,128)(2,1)} async-done(((bf16[192,8,128]{2,0,1:T(8,128)(2,1)}), bf16[1536,8,128]{2,0,1:T(8,128)(2,1)}) %all-gather.4.cloned.1.call-update) | async-done | bytes 3145744 | tf_op jit(solution)/shard_map/all_gather | solution.py:54
  72.3 3.8 %fusion.56 = (bf16[1536,4,128]{2,0,1:T(8,128)(2,1)}, bf16[1536,4,128]{2,0,1:T(8,128)(2,1)}) fusion(bf16[1536,8,128]{2,0,1:T(8,128)(2,1)} %all-gather.4.cloned.1.call-done), kind=kLoop, calls=%fused_computation.102 | loop fusion | bytes 6291456 | tf_op jit(solution)/shard_map/split | solution.py:53
  76.1 2.6 copy.31
  78.7 2.7 copy.32
  81.5 8.9 %while.23 = (s32[]{:T(128)}, f32[4,192]{1,0:T(4,128)S(1)}, f32[4,192]{1,0:T(4,128)S(1)}, f32[4,192,128]{2,1,0:T(8,128)S(1)}, f32[4,192]{1,0:T(4,128)S(1)}, /*ind...) while((s32[]{:T(128)}, f32[4,192]{1,0:T(4,128)S(1)}, ...), condition=%wide.region_7.8_spmd.clone, body=%wide.region_0.7_spmd.clone.sunk | while | flops 309574784 | bytes 20891532 | solution.py:96
  81.5 0.6 dynamic_slice.42
  82.8 5.0 %conditional.3 = ((f32[4,192]{1,0:T(4,128)S(1)}, f32[4,192]{1,0:T(4,128)S(1)}, f32[4,192,128]{2,1,0:T(8,128)S(1)}, f32[4,192]{1,0:T(4,128)S(1)}, f32[4,192]{1,0:T(4,128)S(1)}, /*index=5*/f32[4,192,128]{2,1,0:T(8,128)S(1)})) conditional(s32[]{:T(128)} %convert_element_type.82, (f32[4,192]{1,0:T(4,128)S(1)}, f32[4,192]{1,0:T(4,128)S(1)}, ...), branch_computations={%region_1.1_spmd, %region_2.6_spmd.clone} | conditional | flops 309572096 | bytes 20887848 | solution.py:91
  83.0 1.1 dynamic-slice_bitcast_fusion
  84.1 0.6 fusion.54
  84.7 0.6 fusion.55
  85.2 1.2 fusion.5
  86.5 0.2 copy-done.1
  86.6 0.6 convolution_add_fusion
  87.2 0.6 convolution_add_fusion.1
  87.8 0.6 dynamic_slice.42
  89.2 0.6 dynamic_slice.42
  90.5 0.5 multiply_reduce_fusion.2
  91.0 0.2 multiply_convert_fusion.2
  91.2 8.6 %all_gather.13 = bf16[16,192,128]{2,1,0:T(8,128)(2,1)S(1)} all-gather(bf16[4,192,128]{2,1,0:T(8,128)(2,1)S(1)} %multiply_convert_fusion.2), channel_id=1, replica_groups=mesh['sp'=8,'tp'=4] {'tp'}, dimensions={0}, use_global_device_ids=true | all-gather | bytes 983040 | tf_op jit(solution)/shard_map/all_gather | solution.py:111
  99.8 0.7 multiply_reduce_fusion.1
  100.4 6.2 %psum.7 = f32[192]{0:T(256)S(1)} all-reduce(f32[192]{0:T(256)S(1)} %get-tuple-element.469), channel_id=1, replica_groups=mesh['sp'=8,'tp'=4] {'tp'}, use_global_device_ids=true, to_apply=%region_10.11 | all-reduce | flops 192 | bytes 1536 | tf_op jit(solution)/shard_map/psum | solution.py:118
  106.7 3.3 %gather_fusion = bf16[768,512]{1,0:T(8,128)(2,1)} fusion(bf16[193,512]{1,0:T(8,128)(2,1)S(1)} %concatenate.7, s32[1024]{0:T(1024)S(1)} %pad_clamp_fusion.1), kind=kCustom, calls=%fused_computation | custom fusion | bytes 1575936 | tf_op jit(solution)/shard_map/gather | solution.py:138
  110.1 33.0 %all_to_all.10 = bf16[8,96,512]{2,1,0:T(8,128)(2,1)} all-to-all(bf16[8,96,512]{2,1,0:T(8,128)(2,1)} %bitcast.64), channel_id=1, replica_groups=mesh['sp'=8,'tp'=4] {'sp'}, dimensions={0} | all-to-all | bytes 1572864 | tf_op jit(solution)/shard_map/all_to_all | solution.py:140
  143.1 0.2 all-gather.8.cloned.1.call-start
  143.4 26.8 %all-gather.6.cloned.1.call-done = bf16[8,96,2048]{2,1,0:T(8,128)(2,1)} async-done(((bf16[8,96,512]{2,1,0:T(8,128)(2,1)}), bf16[8,96,2048]{2,1,0:T(8,128)(2,1)}) %all-gather.6.cloned.1.call-update) | async-done | bytes 3145744 | tf_op jit(solution)/shard_map/all_gather | solution.py:139
  170.1 6.3 %fusion.32 = f32[768,1024]{1,0:T(8,128)S(1)} fusion(bf16[768,2048]{1,0:T(8,128)(2,1)} %bitcast.67, bf16[1,2048,1024]{2,1,0:T(8,128)(2,1)} %param.26), kind=kOutput, calls=%fused_computation.55 | convolution fusion | flops 3221225472 | bytes 10485760 | tf_op jit(solution)/shard_map/dot_general | solution.py:149
  176.4 5.3 %multiply_convert_fusion = bf16[768,1024]{1,0:T(8,128)(2,1)} fusion(f32[768,1024]{1,0:T(8,128)S(1)} %fusion.32, bf16[768,2048]{1,0:T(8,128)(2,1)S(1)} %bitcast.68, bf16[1,2048,1024]{2,1,0:T(8,128)(2,1)S(1)} %copy-done.8), kind=kOutput, calls=%fused_computation.59 | convolution fusion | flops 3229089792 | bytes 12058624 | tf_op jit(solution)/shard_map/dot_general | solution.py:148
  181.8 46.5 %all-gather.8.cloned.1.call-done = bf16[768,4096]{1,0:T(8,128)(2,1)} async-done(((bf16[768,1024]{1,0:T(8,128)(2,1)}), bf16[768,4096]{1,0:T(8,128)(2,1)}) %all-gather.8.cloned.1.call-update) | async-done | bytes 6291472 | tf_op jit(solution)/shard_map/all_gather | solution.py:155
  228.3 8.3 %fusion.38 = bf16[768,512]{1,0:T(8,128)(2,1)} fusion(bf16[768,4096]{1,0:T(8,128)(2,1)} %all-gather.8.cloned.1.call-done, bf16[1,4096,512]{2,1,0:T(8,128)(2,1)} %param.27), kind=kOutput, calls=%fused_computation.60 | convolution fusion | flops 3221618688 | bytes 11272192 | tf_op jit(solution)/shard_map/dot_general | solution.py:154
  236.6 5.6 %all-to-all-start.1 = ((bf16[8,96,512]{2,1,0:T(8,128)(2,1)}), bf16[8,96,512]{2,1,0:T(8,128)(2,1)S(1)}, u32[]{:S(2)}, u32[]{:S(2)}) async-start(bf16[8,96,512]{2,1,0:T(8,128)(2,1)} %bitcast.65), calls=%async_computation.1 | async-start | bytes 1572864 | tf_op jit(solution)/shard_map/all_to_all | solution.py:160
  242.4 20.4 %all-to-all-done.1 = bf16[8,96,512]{2,1,0:T(8,128)(2,1)S(1)} async-done(((bf16[8,96,512]{2,1,0:T(8,128)(2,1)}), bf16[8,96,512]{2,1,0:T(8,128)(2,1)S(1)}, u32[]{:S(2)}, u32[]{:S(2)}) %all-to-all-start.1) | async-done | bytes 786464 | tf_op jit(solution)/shard_map/all_to_all | solution.py:160
  262.8 2.6 gather_fusion.1
  265.4 1.5 reshape.153
  266.9 1.0 multiply_reduce_fusion
  267.9 0.7 add_convert_fusion
  (73 shorter events, 1.3 us)
Async XLA Ops:
  6.5 93.2 %copy-start = (bf16[2048,512]{1,0:T(8,128)(2,1)S(1)}, bf16[2048,512]{1,0:T(8,128)(2,1)}, u32[]{:S(2)}) copy-start(bf16[2048,512]{1,0:T(8,128)(2,1)} %param.23) | copy-start | bytes 6291460
  6.5 2.9 %copy-start.5 = (s32[192,2]{0,1:T(2,128)S(1)}, s32[192,2]{0,1:T(2,128)}, u32[]{:S(2)}) copy-start(s32[192,2]{0,1:T(2,128)} %param.28) | copy-start | bytes 4612
  6.5 3.4 %copy-start.2 = (bf16[192,4,128]{2,1,0:T(4,128)(2,1)S(1)}, bf16[192,4,128]{2,1,0:T(4,128)(2,1)}, u32[]{:S(2)}) copy-start(bf16[192,4,128]{2,1,0:T(4,128)(2,1)} %param.18) | copy-start | bytes 589828
  6.5 65.8 %all-gather.4.cloned.1.call-start = ((), (), s32[]{:S(2)}) async-start(), calls=%async_computation.2 | async-start | bytes 3538944 | tf_op jit(solution)/shard_map/all_gather | solution.py:54
  9.4 160.7 %all-gather.6.cloned.1.call-start = ((), (), s32[]{:S(2)}) async-start(), calls=%async_computation.3 | async-start | bytes 3932160 | tf_op jit(solution)/shard_map/all_gather | solution.py:139
  81.5 9.0 %copy-start.6 = (f32[4]{0:T(128)S(1)}, f32[4]{0:T(128)}, u32[]{:S(2)}) copy-start(f32[4]{0:T(128)} %param.21) | copy-start | bytes 52
  81.5 9.5 %copy-start.7 = (f32[128]{0:T(128)S(1)}, f32[128]{0:T(128)}, u32[]{:S(2)}) copy-start(f32[128]{0:T(128)} %param.22) | copy-start | bytes 1540
  85.2 1.4 copy-start.1
  90.5 9.3 %copy-start.3 = (bf16[192,512]{1,0:T(8,128)(2,1)S(1)}, bf16[192,512]{1,0:T(8,128)(2,1)}, u32[]{:S(2)}) copy-start(bf16[192,512]{1,0:T(8,128)(2,1)} %param.17) | copy-start | bytes 589828
  143.1 85.2 %all-gather.8.cloned.1.call-start = ((), (), s32[]{:S(2)}) async-start(), calls=%async_computation.4 | async-start | bytes 7864320 | tf_op jit(solution)/shard_map/all_gather | solution.py:155
  170.1 6.3 %copy-start.8 = (bf16[1,2048,1024]{2,1,0:T(8,128)(2,1)S(1)}, bf16[1,2048,1024]{2,1,0:T(8,128)(2,1)}, u32[]{:S(2)}) copy-start(bf16[1,2048,1024]{2,1,0:T(8,128)(2,1)} %param.25) | copy-start | bytes 12582916
  170.1 6.3 %copy-start.9 = (bf16[8,96,2048]{2,1,0:T(8,128)(2,1)S(1)}, bf16[8,96,2048]{2,1,0:T(8,128)(2,1)}, u32[]{:S(2)}) copy-start(bf16[8,96,2048]{2,1,0:T(8,128)(2,1)} %all-gather.6.cloned.1.call-done) | copy-start | bytes 9437188
  236.6 5.6 %copy-start.4 = (f32[192,2]{0,1:T(2,128)S(1)}, f32[192,2]{0,1:T(2,128)}, u32[]{:S(2)}) copy-start(f32[192,2]{0,1:T(2,128)} %param.29) | copy-start | bytes 4612
  236.6 26.2 %all-to-all-start.1 = ((bf16[8,96,512]{2,1,0:T(8,128)(2,1)}), bf16[8,96,512]{2,1,0:T(8,128)(2,1)S(1)}, u32[]{:S(2)}, u32[]{:S(2)}) async-start(bf16[8,96,512]{2,1,0:T(8,128)(2,1)} %bitcast.65), calls=%async_computation.1 | async-start | bytes 1572864 | tf_op jit(solution)/shard_map/all_to_all | solution.py:160
Sparse Core Ops, SparseCore 0:
  9.5 62.7 all-gather.3
  143.2 26.8 all-gather.5
  181.9 46.3 all-gather.7
